TPU v7x, 32 devices: a whole 2x2x4 slice. The times are simulated.
32 devices in a mesh: ep: 8 (over z, core), tp: 4 (over y, x).
Axes of the slice: x: 2, y: 2, z: 4, core: 2. Of those that a mesh axis runs over, the one named last changes fastest.
Arguments:
- reception_vectors: bfloat16 [1024, 2048], P('ep', 'tp'), may hold values from -6 to 6
- lookup_vectors: bfloat16 [1024, 2048], P('ep', 'tp'), may hold values from -0.75 to 0.75
- payload_vectors: bfloat16 [1024, 2048], P('ep', 'tp'), may hold values from -6 to 6
- fix_strength_signal: bfloat16 [1024, 2048], P('ep', 'tp'), may hold values from -5 to 5
- fade_signal_term: bfloat16 [1024, 2048], P('ep', 'tp'), may hold values from -8 to 8
- state_erasure: bfloat16 [1024, 2048], P('ep', 'tp'), may hold values from 0 to 1
- feature_speed_pairs: float32 [2, 2048], P(None, 'tp'), as said below
- subspace_scale_vector: float32 [2048], P('tp'), may hold values from 0.1 to 1.9
- subspace_merge_matrix: bfloat16 [2048, 4096], P(None, 'tp'), may hold values from -0.125 to 0.125
- specialist_entry_vectors: bfloat16 [512, 4096], P('ep'), may hold values from -6 to 6
- specialist_entry_scale: float32 [4096], replicated, may hold values from 0.1 to 1.9
- specialist_picks: int32 [512, 2], P('ep'), may hold values from 0 to 7, as said below
- dispatch_replica_share: float32 [512, 2], P('ep'), may hold values from 0.2 to 1
- specialist_valve_matrix: bfloat16 [8, 4096, 2048], P('ep', None, 'tp'), may hold values from -0.09375 to 0.09375
- specialist_raising_matrix: bfloat16 [8, 4096, 2048], P('ep', None, 'tp'), may hold values from -0.09375 to 0.09375
- specialist_lowering_matrix: bfloat16 [8, 2048, 4096], P('ep', None, 'tp'), may hold values from -0.125 to 0.125
Outputs:
- sequence_blend_result: bfloat16 [1024, 4096], P('ep', 'tp')
- expert_out: bfloat16 [512, 4096], P('ep', 'tp')
Inputs may be any that keep to these rules, and one draw needn't show every extreme that they name: `specialist_picks`: the two experts of a row differ and lie in one group, experts g * 2 to g * 2 + 1 for some g. Among the rows of one device (aligned blocks of 64 rows) no expert is named more than 24 times, and some expert exactly 24 times. `feature_speed_pairs`: Finite.
All inputs are finite; a program needn't handle non-finite values.
Results may differ from a plain program's by a relative error of at most 0.0071.
Values may be sent and summed in bfloat16 or wider, within the bound.
A program may use at most 128 MiB of HBM per device.

v0:
```python
import jax
import jax.numpy as jnp
from jax import lax
from jax.experimental import pallas as pl
from jax.experimental.pallas import tpu as pltpu
from jax.sharding import PartitionSpec as P

HEAD = 64
GROUPS = 4


highest = lax.Precision.HIGHEST
BLOCK = 256


def split_pair(x):
    high = x.astype(jnp.bfloat16)
    return high, (x - high.astype(jnp.float32)).astype(jnp.bfloat16)


def dot_split(x, y, dims):
    x_high, x_low = split_pair(x)
    y_high, y_low = split_pair(y)

    def one(p, q):
        return lax.dot_general(p, q, (dims, ((), ())), preferred_element_type=jnp.float32)

    return one(x_high, y_high) + (one(x_high, y_low) + one(x_low, y_high))


ROWS = ((1,), (0,))
LAST = ((1,), (1,))
FIRST = ((0,), (0,))


def local_kernel(r_ref, k_ref, v_ref, fix_ref, fade_ref, loss_ref, speed_ref, own_ref, pair_ref):
    span, width = r_ref.shape
    heads = width // HEAD
    levels = span.bit_length() - 1
    decay = jnp.exp(
        -jnp.exp(speed_ref[0:1, :] + fade_ref[...].astype(jnp.float32))
        - loss_ref[...].astype(jnp.float32)
    )
    learn = jax.nn.sigmoid(fix_ref[...].astype(jnp.float32) + speed_ref[1:2, :])
    recept = r_ref[...].astype(jnp.float32)
    key = k_ref[...].astype(jnp.float32)
    squares = key * key
    lane_head = lax.broadcasted_iota(jnp.int32, (span, width), 1) // HEAD
    inverse = jnp.zeros((span, width), jnp.float32)
    for h in range(heads):
        mine = lane_head == h
        total = jnp.sum(jnp.where(mine, squares, 0.0), axis=1, keepdims=True)
        inverse = jnp.where(mine, lax.rsqrt(total + 1e-06), inverse)
    unit = key * inverse
    removal = unit * learn
    place = lax.broadcasted_iota(jnp.int32, (span, width), 0)
    row = lax.broadcasted_iota(jnp.int32, (2 * span, 2 * span), 0) % span
    col = lax.broadcasted_iota(jnp.int32, (2 * span, 2 * span), 1) % span
    small_row = lax.broadcasted_iota(jnp.int32, (span, span), 0)
    small_col = lax.broadcasted_iota(jnp.int32, (span, span), 1)
    eye = jnp.where(small_row == small_col, 1.0, 0.0)
    prefix, before, suffix, total = decay, jnp.ones_like(decay), jnp.ones_like(decay), decay
    scores = [jnp.zeros((2 * span, 2 * span), jnp.float32) for _ in range(heads)]
    solve = [eye for _ in range(heads)]
    for level in range(levels):
        size = 1 << level
        x_unit, x_recept = unit * before, recept * prefix
        y_key, y_removal = key * suffix, removal * suffix
        mask = (
            ((row >> (level + 1)) == (col >> (level + 1)))
            & (((row >> level) & 1) == 1)
            & (((col >> level) & 1) == 0)
        )
        parts = []
        for h in range(heads):
            cut = slice(h * HEAD, (h + 1) * HEAD)
            x = jnp.concatenate([x_unit[:, cut], x_recept[:, cut]], axis=0)
            y = jnp.concatenate([y_key[:, cut], y_removal[:, cut]], axis=0)
            part = jnp.where(mask, dot_split(x, y, LAST), 0.0)
            scores[h] = scores[h] + part
            parts.append(part[:span, span:])
        if level == 0:
            solve = [eye - part for part in parts]
        else:
            half = [dot_split(m, part, ROWS) for m, part in zip(solve, parts)]
            solve = [m - dot_split(q, m, ROWS) for m, q in zip(solve, half)]
        later = ((place >> level) & 1) == 1
        sibling = jnp.where(
            later, pltpu.roll(total, size, 0), pltpu.roll(total, span - size, 0)
        )
        prefix = jnp.where(later, prefix * sibling, prefix)
        before = jnp.where(later, before * sibling, before)
        suffix = jnp.where(later, suffix, suffix * sibling)
        total = total * sibling
    x_unit, x_recept = unit * before, recept * prefix
    y_key, y_removal = key * suffix, removal * suffix
    value = v_ref[...].astype(jnp.float32)
    same = recept * key
    taken = recept * removal
    head_eye = jnp.where(
        lax.broadcasted_iota(jnp.int32, (HEAD, HEAD), 0)
        == lax.broadcasted_iota(jnp.int32, (HEAD, HEAD), 1),
        1.0,
        0.0,
    )
    for h in range(heads):
        cut = slice(h * HEAD, (h + 1) * HEAD)
        both = scores[h]
        value_h = value[:, cut]
        same_h = jnp.sum(same[:, cut], axis=1, keepdims=True)
        taken_h = jnp.sum(taken[:, cut], axis=1, keepdims=True)
        from_value = dot_split(both[:, :span], value_h, ROWS)
        right = jnp.concatenate([from_value[:span], x_unit[:, cut]], axis=1)
        hit = dot_split(solve[h], right, ROWS)
        left = jnp.concatenate([from_value[span:] + same_h * value_h, x_recept[:, cut]], axis=1)
        left = left - dot_split(both[span:, span:], hit, ROWS) - taken_h * hit
        own_ref[:, 2 * h * HEAD : 2 * (h + 1) * HEAD] = left
        change = jnp.concatenate(
            [dot_split(value_h, y_key[:, cut], FIRST), head_eye * total[0:1, cut]], axis=0
        )
        pair_ref[:, cut] = change - dot_split(hit, y_removal[:, cut], FIRST)


def local_part(arrays, speeds):
    span, channels = arrays[0].shape
    width = min(channels, BLOCK)
    spec = pl.BlockSpec((span, width), lambda i: (0, i))
    return pl.pallas_call(
        local_kernel,
        grid=(channels // width,),
        in_specs=[spec] * 6 + [pl.BlockSpec((2, width), lambda i: (0, i))],
        out_specs=[
            pl.BlockSpec((span, 2 * width), lambda i: (0, i)),
            pl.BlockSpec((2 * HEAD, width), lambda i: (0, i)),
        ],
        out_shape=[
            jax.ShapeDtypeStruct((span, 2 * channels), jnp.float32),
            jax.ShapeDtypeStruct((2 * HEAD, channels), jnp.float32),
        ],
        cost_estimate=pl.CostEstimate(
            flops=channels * span * span * 40, bytes_accessed=span * channels * 26, transcendentals=0
        ),
        name="local_part",
    )(*arrays, speeds)


def finish_kernel(own_ref, pairs_ref, scale_ref, out_ref):
    span, channels = out_ref.shape
    heads = channels // HEAD
    place = lax.axis_index("ep")

    def one(step, states):
        after = []
        for h, state in enumerate(states):
            cut = slice(h * HEAD, (h + 1) * HEAD)
            later = pairs_ref[step, HEAD:, cut]
            after.append(dot_split(state, later, ROWS) + pairs_ref[step, :HEAD, cut])
        return tuple(after)

    zero = jnp.zeros((HEAD, HEAD), jnp.float32)
    states = lax.fori_loop(0, place, one, tuple(zero for _ in range(heads)))
    for h, state in enumerate(states):
        cut = slice(h * HEAD, (h + 1) * HEAD)
        own = own_ref[:, 2 * h * HEAD : (2 * h + 1) * HEAD]
        carried = own_ref[:, (2 * h + 1) * HEAD : 2 * (h + 1) * HEAD]
        out = own + dot_split(carried, state, LAST)
        centred = out - jnp.mean(out, axis=1, keepdims=True)
        var = jnp.mean(centred * centred, axis=1, keepdims=True)
        out_ref[:, cut] = (centred * lax.rsqrt(var + 0.00064) * scale_ref[0:1, cut]).astype(
            jnp.bfloat16
        )


def finish_part(own, pairs, scale):
    span, channels = own.shape[0], own.shape[1] // 2
    return pl.pallas_call(
        finish_kernel,
        out_shape=jax.ShapeDtypeStruct((span, channels), jnp.bfloat16),
        name="finish_part",
    )(own, pairs, scale)


def blend_sequence(
    reception_vectors,
    lookup_vectors,
    payload_vectors,
    fix_strength_signal,
    fade_signal_term,
    state_erasure,
    feature_speed_pairs,
    subspace_scale_vector,
    subspace_merge_matrix,
):
    own, pair = local_part(
        (
            reception_vectors,
            lookup_vectors,
            payload_vectors,
            fix_strength_signal,
            fade_signal_term,
            state_erasure,
        ),
        feature_speed_pairs,
    )
    pairs = lax.all_gather(pair, "ep")
    mixed_rows = finish_part(own, pairs, subspace_scale_vector.reshape(1, -1))
    return jnp.dot(
        lax.all_gather(mixed_rows, "tp", axis=1, tiled=True),
        subspace_merge_matrix,
        preferred_element_type=jnp.float32,
    ).astype(jnp.bfloat16)


def expert_layer(
    specialist_entry_vectors,
    specialist_entry_scale,
    specialist_picks,
    dispatch_replica_share,
    specialist_valve_matrix,
    specialist_raising_matrix,
    specialist_lowering_matrix,
):
    rows_here, model_width = specialist_entry_vectors.shape
    pairs = specialist_picks.shape[1]
    expert_count = lax.axis_size("ep") * specialist_valve_matrix.shape[0]
    per_group = expert_count // GROUPS
    busiest = per_group * max(1, 3 * rows_here // (8 * per_group))
    capacity = 2 * busiest // per_group
    widened = specialist_entry_vectors.astype(jnp.float32)
    normed = (
        widened
        * lax.rsqrt(jnp.mean(widened * widened, axis=-1, keepdims=True) + 1e-06)
        * specialist_entry_scale
    ).astype(jnp.bfloat16)
    flat_ids = specialist_picks.reshape(-1)
    onehot = (flat_ids[:, None] == jnp.arange(expert_count, dtype=jnp.int32)[None, :]).astype(
        jnp.int32
    )
    slot_rank = jnp.sum((jnp.cumsum(onehot, axis=0) - onehot) * onehot, axis=1)
    slot_index = flat_ids * capacity + slot_rank
    selected = jnp.arange(expert_count * capacity, dtype=jnp.int32)[:, None] == slot_index[None, :]
    selected = selected.reshape(expert_count * capacity, rows_here, pairs)
    placement_mat = jnp.any(selected, axis=-1).astype(jnp.bfloat16)
    combine_w = jnp.sum(selected.astype(jnp.float32) * dispatch_replica_share[None], axis=-1)
    send_rows = jnp.dot(placement_mat, normed, preferred_element_type=jnp.float32).astype(
        jnp.bfloat16
    )
    send_rows = send_rows.reshape(expert_count, capacity, model_width)
    arrived = lax.all_to_all(send_rows, "ep", split_axis=0, concat_axis=0, tiled=True)
    sources, item_count, feature_count = arrived.shape
    flat_rows = arrived.reshape(sources * item_count, feature_count)
    gate_part = jnp.dot(flat_rows, specialist_valve_matrix[0], preferred_element_type=jnp.float32)
    up_part = jnp.dot(flat_rows, specialist_raising_matrix[0], preferred_element_type=jnp.float32)
    hidden = (jax.nn.silu(gate_part) * up_part).astype(jnp.bfloat16)
    weight_rows = specialist_lowering_matrix[0]
    result = jnp.dot(
        lax.all_gather(hidden, "tp", axis=1, tiled=True),
        weight_rows,
        preferred_element_type=jnp.float32,
    ).astype(jnp.bfloat16)
    result = result.reshape(sources, item_count, specialist_lowering_matrix.shape[2])
    returned = lax.all_to_all(result, "ep", split_axis=0, concat_axis=0, tiled=True)
    flat_back = returned.reshape(expert_count * capacity, returned.shape[2]).astype(jnp.float32)
    combined = jnp.einsum("st,sd->td", combine_w, flat_back, precision=highest)
    return combined.astype(jnp.bfloat16)


def body(
    reception_vectors,
    lookup_vectors,
    payload_vectors,
    fix_strength_signal,
    fade_signal_term,
    state_erasure,
    feature_speed_pairs,
    subspace_scale_vector,
    subspace_merge_matrix,
    specialist_entry_vectors,
    specialist_entry_scale,
    specialist_picks,
    dispatch_replica_share,
    specialist_valve_matrix,
    specialist_raising_matrix,
    specialist_lowering_matrix,
):
    sequence_blend_result = blend_sequence(
        reception_vectors,
        lookup_vectors,
        payload_vectors,
        fix_strength_signal,
        fade_signal_term,
        state_erasure,
        feature_speed_pairs,
        subspace_scale_vector,
        subspace_merge_matrix,
    )
    expert_out = expert_layer(
        specialist_entry_vectors,
        specialist_entry_scale,
        specialist_picks,
        dispatch_replica_share,
        specialist_valve_matrix,
        specialist_raising_matrix,
        specialist_lowering_matrix,
    )
    return (sequence_blend_result, expert_out)


def solution(mesh):
    placed = (
        P("ep", "tp"),
        P("ep", "tp"),
        P("ep", "tp"),
        P("ep", "tp"),
        P("ep", "tp"),
        P("ep", "tp"),
        P(None, "tp"),
        P("tp"),
        P(None, "tp"),
        P("ep", None),
        P(),
        P("ep", None),
        P("ep", None),
        P("ep", None, "tp"),
        P("ep", None, "tp"),
        P("ep", None, "tp"),
    )
    return jax.shard_map(
        body, mesh=mesh, in_specs=placed, out_specs=(P("ep", "tp"), P("ep", "tp")), check_vma=False
    )
```

profile of v0, /device:TPU:0, one launch (start us, length us, event | category | flops | bytes accessed | tf_op | source)
XLA Modules:
  0.0 133.6 jit_solution(5923044101234514603)
XLA Ops:
  7.2 0.8 copy.30
  7.9 0.1 eq.30
  8.1 0.1 fusion.22
  8.2 0.2 reduce_window_sum.11
  8.3 0.2 select_reduce_fusion.1
  8.5 0.1 reduce_sum.30
  8.7 0.1 copy.31
  8.7 0.7 multiply_add_fusion
  9.4 0.1 fusion.21
  9.5 1.2 fusion.15
  10.8 2.8 %convolution_convert_fusion = bf16[192,4096]{1,0:T(8,128)(2,1)} fusion(pred[192,64]{0,1:T(8,128)(4,1)S(1)} %fusion.21, bf16[64,4096]{1,0:T(8,128)(2,1)} %param.25, f32[4096]{0:T(1024)} %param.26, f32[64]{0:T(128)S(1)} %add_rsqrt_fusion), kind=kOutput, calls=%fused_computation | convolution fusion | flops 102498304 | bytes 2126080 | tf_op jit(solution)/shard_map/dot_general | solution.py:245
  13.6 6.4 %all-to-all-start = ((bf16[8,24,4096]{2,1,0:T(8,128)(2,1)}), bf16[8,24,4096]{2,1,0:T(8,128)(2,1)S(1)}, u32[]{:S(2)}, u32[]{:S(2)}) async-start(bf16[8,24,4096]{2,1,0:T(8,128)(2,1)} %bitcast.2), calls=%async_computation | async-start | bytes 3145728 | tf_op jit(solution)/shard_map/all_to_all | solution.py:249
  20.0 0.0 all-gather.3.cloned.1.call-start
  20.0 16.5 %local_part.1 = (f32[128,1024]{1,0:T(8,128)}, f32[128,512]{1,0:T(8,128)}) custom-call(bf16[128,512]{1,0:T(8,128)(2,1)} %r_ref.1, bf16[128,512]{1,0:T(8,128)(2,1)} %k_ref.1, bf16[128,512]{1,0:T(8,128)(2,1)} %v_ref.1, bf16[128,512]{1,0:T(8,128)(2,1)} %fix_ref.1, bf16[128,512]{1,0:T(8,128)(2,1)} %fade_ref.1, bf16[128,512]{1,0:T(8,128)(2,1)} %loss_ref.1, ...), custom_call_target="tpu_custom_call" | custom-call | flops 335544320 | bytes 1703936 | tf_op jit(solution)/shard_map/local_part/pallas_call | solution.py:128
  36.5 0.0 all-gather.3.cloned.1.call-update
  36.6 37.6 %all-to-all-done = bf16[8,24,4096]{2,1,0:T(8,128)(2,1)S(1)} async-done(((bf16[8,24,4096]{2,1,0:T(8,128)(2,1)}), bf16[8,24,4096]{2,1,0:T(8,128)(2,1)S(1)}, u32[]{:S(2)}, u32[]{:S(2)}) %all-to-all-start) | async-done | bytes 1572896 | tf_op jit(solution)/shard_map/all_to_all | solution.py:249
  74.2 0.0 copy-start.1
  74.2 3.3 %fusion.4 = f32[192,512]{1,0:T(8,128)S(1)} fusion(bf16[192,4096]{1,0:T(8,128)(2,1)S(1)} %bitcast.29, bf16[1,4096,512]{2,1,0:T(8,128)(2,1)} %param.29), kind=kOutput, calls=%fused_computation.5 | convolution fusion | flops 805306368 | bytes 6160384 | tf_op jit(solution)/shard_map/dot_general | solution.py:252
  77.5 0.2 copy-done.1
  77.7 0.0 copy-start.2
  77.7 1.0 fusion.12
  78.7 0.0 copy-start
  78.7 11.5 %all_gather.15 = bf16[192,2048]{1,0:T(8,128)(2,1)S(1)} all-gather(bf16[192,512]{1,0:T(8,128)(2,1)S(1)} %fusion.12), channel_id=1, replica_groups=mesh['ep'=8,'tp'=4] {'tp'}, dimensions={1}, use_global_device_ids=true | all-gather | bytes 983040 | tf_op jit(solution)/shard_map/all_gather | solution.py:257
  90.2 0.0 copy-done.2
  90.2 1.8 %fusion.6 = bf16[192,1024]{1,0:T(8,128)(2,1)} fusion(bf16[192,2048]{1,0:T(8,128)(2,1)S(1)} %all_gather.15, bf16[1,2048,1024]{2,1,0:T(8,128)(2,1)S(1)} %copy-done.2), kind=kOutput, calls=%fused_computation.9 | convolution fusion | flops 805502976 | bytes 5373952 | tf_op jit(solution)/shard_map/dot_general | solution.py:256
  92.0 3.5 %all-to-all-start.1 = ((bf16[8,24,1024]{2,1,0:T(8,128)(2,1)}), bf16[8,24,1024]{2,1,0:T(8,128)(2,1)S(1)}, u32[]{:S(2)}, u32[]{:S(2)}) async-start(bf16[8,24,1024]{2,1,0:T(8,128)(2,1)} %bitcast.7), calls=%async_computation.1 | async-start | bytes 786432 | tf_op jit(solution)/shard_map/all_to_all | solution.py:262
  95.5 0.0 copy-done
  95.5 0.1 select_reduce_fusion
  95.6 12.4 %all-to-all-done.1 = bf16[8,24,1024]{2,1,0:T(8,128)(2,1)S(1)} async-done(((bf16[8,24,1024]{2,1,0:T(8,128)(2,1)}), bf16[8,24,1024]{2,1,0:T(8,128)(2,1)S(1)}, u32[]{:S(2)}, u32[]{:S(2)}) %all-to-all-start.1) | async-done | bytes 393248 | tf_op jit(solution)/shard_map/all_to_all | solution.py:262
  108.0 1.0 convolution_convert_fusion.2
  109.0 0.0 all-gather.3.cloned.1.call-done
  109.0 3.5 %finish_part.1 = bf16[128,512]{1,0:T(8,128)(2,1)} custom-call(f32[128,1024]{1,0:T(8,128)} %get-tuple-element.4.own_ref, f32[8,128,512]{2,1,0:T(8,128)} %bitcast.31, f32[1,512]{1,0:T(1,128)} %bitcast.33), custom_call_target="tpu_custom_call" | custom-call | tf_op jit(solution)/shard_map/finish_part/pallas_call | solution.py:176
  112.5 10.7 %all_gather.14 = bf16[128,2048]{1,0:T(8,128)(2,1)S(1)} all-gather(bf16[128,512]{1,0:T(8,128)(2,1)} %finish_part.1), channel_id=1, replica_groups=mesh['ep'=8,'tp'=4] {'tp'}, dimensions={1}, use_global_device_ids=true | all-gather | bytes 655360 | tf_op jit(solution)/shard_map/all_gather | solution.py:208
  123.1 3.7 %convolution_convert_fusion.1 = bf16[128,1024]{1,0:T(8,128)(2,1)} fusion(bf16[128,2048]{1,0:T(8,128)(2,1)S(1)} %all_gather.14, bf16[2048,1024]{1,0:T(8,128)(2,1)} %param.24), kind=kOutput, calls=%fused_computation.11 | convolution fusion | flops 537001984 | bytes 4980736 | tf_op jit(solution)/shard_map/dot_general | solution.py:207
  (1 shorter events, 0.0 us)
Async XLA Ops:
  13.6 60.5 %all-to-all-start = ((bf16[8,24,4096]{2,1,0:T(8,128)(2,1)}), bf16[8,24,4096]{2,1,0:T(8,128)(2,1)S(1)}, u32[]{:S(2)}, u32[]{:S(2)}) async-start(bf16[8,24,4096]{2,1,0:T(8,128)(2,1)} %bitcast.2), calls=%async_computation | async-start | bytes 3145728 | tf_op jit(solution)/shard_map/all_to_all | solution.py:249
  20.0 89.0 %all-gather.3.cloned.1.call-start = ((), (), s32[]{:S(2)}) async-start(), calls=%async_computation.2 | async-start | bytes 2359296 | tf_op jit(solution)/shard_map/all_gather | solution.py:205
  74.2 3.5 %copy-start.1 = (bf16[1,4096,512]{2,1,0:T(8,128)(2,1)S(1)}, bf16[1,4096,512]{2,1,0:T(8,128)(2,1)}, u32[]{:S(2)}) copy-start(bf16[1,4096,512]{2,1,0:T(8,128)(2,1)} %param.30) | copy-start | bytes 12582916
  77.7 12.6 %copy-start.2 = (bf16[1,2048,1024]{2,1,0:T(8,128)(2,1)S(1)}, bf16[1,2048,1024]{2,1,0:T(8,128)(2,1)}, u32[]{:S(2)}) copy-start(bf16[1,2048,1024]{2,1,0:T(8,128)(2,1)} %param.31) | copy-start | bytes 12582916
  78.7 16.8 %copy-start = (f32[64,2]{0,1:T(2,128)S(1)}, f32[64,2]{0,1:T(2,128)}, u32[]{:S(2)}) copy-start(f32[64,2]{0,1:T(2,128)} %param.28) | copy-start | bytes 1540
  92.0 16.0 %all-to-all-start.1 = ((bf16[8,24,1024]{2,1,0:T(8,128)(2,1)}), bf16[8,24,1024]{2,1,0:T(8,128)(2,1)S(1)}, u32[]{:S(2)}, u32[]{:S(2)}) async-start(bf16[8,24,1024]{2,1,0:T(8,128)(2,1)} %bitcast.7), calls=%async_computation.1 | async-start | bytes 786432 | tf_op jit(solution)/shard_map/all_to_all | solution.py:262
Sparse Core Ops, SparseCore 0:
  36.7 39.4 all-gather.2
where the time goes:
time: 134 us
  waiting for transfers between devices  50 us (37%)
  blocking collectives  22.2 us (17%)
  Pallas kernels  20 us (15%)
  between operations  14.1 us (11%)
  matrix products  13.6 us (10%)
  starting transfers between devices  9.87 us (7%)
  other arithmetic  2.57 us (2%)
    all_to_all x1, waiting for transfers between devices, expert_layer(): lax.all_to_all(send_rows, 'ep', split_axis=0, concat_axis=0, tiled=True)  37.6 us
    pallas_call x1, Pallas kernels, local_part(): pl.pallas_call(local_kernel, grid=(channels // width,), in_specs=[spec] *...  16.5 us
    all_to_all x1, waiting for transfers between devices, expert_layer(): lax.all_to_all(result, 'ep', split_axis=0, concat_axis=0, tiled=True)  12.4 us
    all_gather x1, blocking collectives, expert_layer(): lax.all_gather(hidden, 'tp', axis=1, tiled=True)  11.5 us
    all_gather x1, blocking collectives, blend_sequence(): lax.all_gather(mixed_rows, 'tp', axis=1, tiled=True)  10.7 us
    all_to_all x1, starting transfers between devices, expert_layer(): lax.all_to_all(send_rows, 'ep', split_axis=0, concat_axis=0, tiled=True)  6.35 us
    dot_general x1, matrix products, blend_sequence(): jnp.dot(lax.all_gather(mixed_rows, 'tp', axis=1, tiled=True), subspace_me...  3.66 us
    all_to_all x1, starting transfers between devices, expert_layer(): lax.all_to_all(result, 'ep', split_axis=0, concat_axis=0, tiled=True)  3.48 us
  transfers between devices with their start and end apart: 3, of which 2 were waited for; matrix products, arithmetic and copies ran while one was open for 5% of the time, Pallas kernels for 12%

commit v1 on v0

--- a/solution.py
+++ b/solution.py
@@ -118,7 +118,8 @@
         change = jnp.concatenate(
             [dot_split(value_h, y_key[:, cut], FIRST), head_eye * total[0:1, cut]], axis=0
         )
-        pair_ref[:, cut] = change - dot_split(hit, y_removal[:, cut], FIRST)
+        change = change - dot_split(hit, y_removal[:, cut], FIRST)
+        pair_ref[:, cut] = change.astype(jnp.bfloat16)
 
 
 def local_part(arrays, speeds):
@@ -135,7 +136,7 @@
         ],
         out_shape=[
             jax.ShapeDtypeStruct((span, 2 * channels), jnp.float32),
-            jax.ShapeDtypeStruct((2 * HEAD, channels), jnp.float32),
+            jax.ShapeDtypeStruct((2 * HEAD, channels), jnp.bfloat16),
         ],
         cost_estimate=pl.CostEstimate(
             flops=channels * span * span * 40, bytes_accessed=span * channels * 26, transcendentals=0
@@ -154,7 +155,11 @@
         for h, state in enumerate(states):
             cut = slice(h * HEAD, (h + 1) * HEAD)
             later = pairs_ref[step, HEAD:, cut]
-            after.append(dot_split(state, later, ROWS) + pairs_ref[step, :HEAD, cut])
+            high, low = split_pair(state)
+            both = jnp.concatenate([high, low], axis=0)
+            moved = jnp.dot(both, later, preferred_element_type=jnp.float32)
+            earned = pairs_ref[step, :HEAD, cut].astype(jnp.float32)
+            after.append(moved[:HEAD] + moved[HEAD:] + earned)
         return tuple(after)
 
     zero = jnp.zeros((HEAD, HEAD), jnp.float32)
@@ -176,8 +181,85 @@
     return pl.pallas_call(
         finish_kernel,
         out_shape=jax.ShapeDtypeStruct((span, channels), jnp.bfloat16),
+        cost_estimate=pl.CostEstimate(
+            flops=pairs.size * HEAD * 8, bytes_accessed=pairs.size * 16, transcendentals=0
+        ),
         name="finish_part",
     )(own, pairs, scale)
+
+
+def collect_kernel(x_ref, out_ref, own_sem, send_sem, recv_sem):
+    members, peers = send_sem.shape
+    depth = x_ref.shape[1]
+    place, column = lax.axis_index("ep"), lax.axis_index("tp")
+    member = lax.rem(place, members)
+    first = place - member
+
+    def peer(step):
+        return {"tp": lax.rem(column + step, peers)}
+
+    def partner(step):
+        return {"ep": first + lax.rem(member + step, members)}
+
+    def block(owner):
+        return out_ref.at[member, :, pl.ds(pl.multiple_of(owner * depth, 128), depth)]
+
+    def send(source, target, m, q, device):
+        copy = pltpu.make_async_remote_copy(
+            src_ref=source,
+            dst_ref=target,
+            send_sem=send_sem.at[m, q],
+            recv_sem=recv_sem.at[m, q],
+            device_id=device,
+            device_id_type=pl.DeviceIdType.MESH,
+        )
+        copy.start()
+        return copy
+
+    barrier = pltpu.get_barrier_semaphore()
+    others = [peer(q) for q in range(1, peers)] + [partner(m) for m in range(1, members)]
+    for device in others:
+        pl.semaphore_signal(
+            barrier, inc=1, device_id=device, device_id_type=pl.DeviceIdType.MESH
+        )
+    pl.semaphore_wait(barrier, len(others))
+    across = [send(x_ref, block(column), 0, q, peer(q)) for q in range(1, peers)]
+    within = [send(x_ref, block(column), m, 0, partner(m)) for m in range(1, members)]
+    mine = pltpu.make_async_copy(x_ref, block(column), own_sem)
+    mine.start()
+    for q in range(1, peers):
+        across[q - 1].wait_recv()
+        landed = block(lax.rem(column + peers - q, peers))
+        for m in range(1, members):
+            within.append(send(landed, landed, m, q, partner(m)))
+    for copy in across:
+        copy.wait_send()
+    for copy in within:
+        copy.wait()
+    mine.wait()
+
+
+def collect(x, members, collective_id, name):
+    rows, depth = x.shape
+    peers = lax.axis_size("tp")
+    return pl.pallas_call(
+        collect_kernel,
+        out_shape=jax.ShapeDtypeStruct((members, rows, peers * depth), x.dtype),
+        in_specs=[pl.BlockSpec(memory_space=pltpu.VMEM)],
+        out_specs=pl.BlockSpec(memory_space=pltpu.VMEM),
+        scratch_shapes=[
+            pltpu.SemaphoreType.DMA,
+            pltpu.SemaphoreType.DMA((members, peers)),
+            pltpu.SemaphoreType.DMA((members, peers)),
+        ],
+        compiler_params=pltpu.CompilerParams(
+            collective_id=collective_id, has_side_effects=True
+        ),
+        cost_estimate=pl.CostEstimate(
+            flops=0, bytes_accessed=16 * x.size * members * peers, transcendentals=0
+        ),
+        name=name,
+    )(x).reshape(members * rows, peers * depth)
 
 
 def blend_sequence(
@@ -191,27 +273,36 @@
     subspace_scale_vector,
     subspace_merge_matrix,
 ):
-    own, pair = local_part(
-        (
-            reception_vectors,
-            lookup_vectors,
-            payload_vectors,
-            fix_strength_signal,
-            fade_signal_term,
-            state_erasure,
-        ),
-        feature_speed_pairs,
-    )
-    pairs = lax.all_gather(pair, "ep")
-    mixed_rows = finish_part(own, pairs, subspace_scale_vector.reshape(1, -1))
-    return jnp.dot(
-        lax.all_gather(mixed_rows, "tp", axis=1, tiled=True),
-        subspace_merge_matrix,
-        preferred_element_type=jnp.float32,
-    ).astype(jnp.bfloat16)
+    def begin(after):
+        after, recept = lax.optimization_barrier((after, reception_vectors))
+        own, pair = local_part(
+            (
+                recept,
+                lookup_vectors,
+                payload_vectors,
+                fix_strength_signal,
+                fade_signal_term,
+                state_erasure,
+            ),
+            feature_speed_pairs,
+        )
+        return after, own, lax.all_gather(pair, "ep")
+
+    def finish(own, pairs, after):
+        ready, _ = lax.optimization_barrier((own, after))
+        mixed_rows = finish_part(ready, pairs, subspace_scale_vector.reshape(1, -1))
+        return jnp.dot(
+            collect(mixed_rows, 1, 3, "mixed_gather"),
+            subspace_merge_matrix,
+            preferred_element_type=jnp.float32,
+        ).astype(jnp.bfloat16)
+
+    return begin, finish
 
 
 def expert_layer(
+    begin,
+    finish,
     specialist_entry_vectors,
     specialist_entry_scale,
     specialist_picks,
@@ -225,44 +316,57 @@
     expert_count = lax.axis_size("ep") * specialist_valve_matrix.shape[0]
     per_group = expert_count // GROUPS
     busiest = per_group * max(1, 3 * rows_here // (8 * per_group))
-    capacity = 2 * busiest // per_group
+    share = busiest // per_group
     widened = specialist_entry_vectors.astype(jnp.float32)
-    normed = (
-        widened
-        * lax.rsqrt(jnp.mean(widened * widened, axis=-1, keepdims=True) + 1e-06)
-        * specialist_entry_scale
-    ).astype(jnp.bfloat16)
-    flat_ids = specialist_picks.reshape(-1)
-    onehot = (flat_ids[:, None] == jnp.arange(expert_count, dtype=jnp.int32)[None, :]).astype(
-        jnp.int32
-    )
-    slot_rank = jnp.sum((jnp.cumsum(onehot, axis=0) - onehot) * onehot, axis=1)
-    slot_index = flat_ids * capacity + slot_rank
-    selected = jnp.arange(expert_count * capacity, dtype=jnp.int32)[:, None] == slot_index[None, :]
-    selected = selected.reshape(expert_count * capacity, rows_here, pairs)
-    placement_mat = jnp.any(selected, axis=-1).astype(jnp.bfloat16)
-    combine_w = jnp.sum(selected.astype(jnp.float32) * dispatch_replica_share[None], axis=-1)
+    inverse = lax.rsqrt(jnp.mean(widened * widened, axis=-1, keepdims=True) + 1e-06)
+    depth = model_width // lax.axis_size("tp")
+    start = lax.axis_index("tp") * depth
+    columns = lax.dynamic_slice_in_dim(specialist_entry_vectors, start, depth, 1)
+    gain = lax.dynamic_slice_in_dim(specialist_entry_scale, start, depth, 0)
+    normed = (columns.astype(jnp.float32) * inverse * gain).astype(jnp.bfloat16)
+    group = specialist_picks[:, 0] // per_group
+    earlier = jnp.arange(rows_here)[:, None] > jnp.arange(rows_here)[None, :]
+    rank = jnp.sum(((group[:, None] == group[None, :]) & earlier).astype(jnp.int32), axis=1)
+    slots = jnp.arange(GROUPS * busiest, dtype=jnp.int32)[:, None]
+    placement_mat = (slots == (group * busiest + rank)[None, :]).astype(jnp.bfloat16)
     send_rows = jnp.dot(placement_mat, normed, preferred_element_type=jnp.float32).astype(
         jnp.bfloat16
     )
-    send_rows = send_rows.reshape(expert_count, capacity, model_width)
+    send_rows = send_rows.reshape(expert_count, share, depth)
+    send_rows, own, pairs = begin(send_rows)
     arrived = lax.all_to_all(send_rows, "ep", split_axis=0, concat_axis=0, tiled=True)
-    sources, item_count, feature_count = arrived.shape
-    flat_rows = arrived.reshape(sources * item_count, feature_count)
+    flat_rows = collect(arrived.reshape(expert_count * share, depth), per_group, 1, "row_gather")
     gate_part = jnp.dot(flat_rows, specialist_valve_matrix[0], preferred_element_type=jnp.float32)
     up_part = jnp.dot(flat_rows, specialist_raising_matrix[0], preferred_element_type=jnp.float32)
     hidden = (jax.nn.silu(gate_part) * up_part).astype(jnp.bfloat16)
-    weight_rows = specialist_lowering_matrix[0]
     result = jnp.dot(
-        lax.all_gather(hidden, "tp", axis=1, tiled=True),
-        weight_rows,
+        collect(hidden, 1, 2, "hidden_gather"),
+        specialist_lowering_matrix[0],
         preferred_element_type=jnp.float32,
     ).astype(jnp.bfloat16)
-    result = result.reshape(sources, item_count, specialist_lowering_matrix.shape[2])
-    returned = lax.all_to_all(result, "ep", split_axis=0, concat_axis=0, tiled=True)
-    flat_back = returned.reshape(expert_count * capacity, returned.shape[2]).astype(jnp.float32)
+    out_width = result.shape[1]
+    result = result.reshape(per_group, expert_count, share, out_width)
+    mixed = finish(own, pairs, result)
+    returned = lax.all_to_all(
+        result.transpose(1, 0, 2, 3).reshape(expert_count, busiest, out_width),
+        "ep",
+        split_axis=0,
+        concat_axis=0,
+        tiled=True,
+    )
+    returned, mixed = lax.optimization_barrier((returned, mixed))
+    flat_back = returned.reshape(expert_count * busiest, out_width).astype(jnp.float32)
+    expert_of = jnp.arange(expert_count, dtype=jnp.int32)[:, None]
+    weight = jnp.sum(
+        jnp.where(
+            specialist_picks[None] == expert_of[:, :, None], dispatch_replica_share[None], 0.0
+        ),
+        axis=-1,
+    )
+    here = jnp.arange(busiest, dtype=jnp.int32)[:, None] == rank[None, :]
+    combine_w = jnp.where(here[None], weight[:, None, :], 0.0).reshape(-1, rows_here)
     combined = jnp.einsum("st,sd->td", combine_w, flat_back, precision=highest)
-    return combined.astype(jnp.bfloat16)
+    return mixed, combined.astype(jnp.bfloat16)
 
 
 def body(
@@ -283,7 +387,7 @@
     specialist_raising_matrix,
     specialist_lowering_matrix,
 ):
-    sequence_blend_result = blend_sequence(
+    begin, finish = blend_sequence(
         reception_vectors,
         lookup_vectors,
         payload_vectors,
@@ -294,7 +398,9 @@
         subspace_scale_vector,
         subspace_merge_matrix,
     )
-    expert_out = expert_layer(
+    return expert_layer(
+        begin,
+        finish,
         specialist_entry_vectors,
         specialist_entry_scale,
         specialist_picks,
@@ -303,7 +409,6 @@
         specialist_raising_matrix,
         specialist_lowering_matrix,
     )
-    return (sequence_blend_result, expert_out)
 
 
 def solution(mesh):

time: 134 us -> 110 us (0.82)
  waiting for transfers between devices: 50 us -> 0.04 us
  Pallas kernels: 20 us -> 61.4 us
  blocking collectives: 22.2 us -> 0 us
  local copies, waits for them, and re-layouts: 1.28 us -> 4.05 us
    pallas_call x0 -> x3, Pallas kernels: none -> 41.7 us  [collect(): pl.pallas_call(collect_kernel, out_shape=jax.ShapeDtypeStruct((members, r...]
    all_to_all x1, waiting for transfers between devices: 37.6 us -> 0.01 us  [expert_layer(): lax.all_to_all(send_rows, 'ep', split_axis=0, concat_axis=0, tiled=True)]
    all_gather x2 -> x0, blocking collectives: 22.2 us -> none  [the longest x1 11.5 us: expert_layer(): lax.all_gather(hidden, 'tp', axis=1, tiled=True)]
    all_to_all x1, waiting for transfers between devices: 12.4 us -> 0.01 us  [expert_layer(): lax.all_to_all(result.transpose(1, 0, 2, 3).reshape(expert_count, busiest...]
    reshape x0 -> x4, local copies, waits for them, and re-layouts: none -> 2.53 us  [the longest x1 0.97 us: expert_layer(): result.transpose(1, 0, 2, 3).reshape(expert_count, busiest, out_width)]
    dot_general x2, matrix products: 5.42 us -> 7.2 us  [the longest x1 3.78 us: finish(): jnp.dot(collect(mixed_rows, 1, 3, 'mixed_gather'), subspace_merge_matrix,...]
    dot_general x1, matrix products: 2.85 us -> 1.17 us  [expert_layer(): jnp.dot(placement_mat, normed, preferred_element_type=jnp.float32)]
  transfers between devices with their start and end apart: 3 -> 3, of which waited for: 2 -> 0; matrix products, arithmetic and copies ran while one was open for 5% -> 13% of each run, Pallas kernels for 12% -> 56%
where the time goes in v1:
time: 110 us; the launch traced here: 109 us
  Pallas kernels  61.4 us (56%)
  matrix products  14.9 us (14%)
  between operations  14.2 us (13%)
  starting transfers between devices  11 us (10%)
  local copies, waits for them, and re-layouts  4.05 us (4%)
  other arithmetic  3.52 us (3%)
    pallas_call x3, Pallas kernels, collect(): pl.pallas_call(collect_kernel, out_shape=jax.ShapeDtypeStruct((members, r...  41.7 us
    pallas_call x1, Pallas kernels, local_part(): pl.pallas_call(local_kernel, grid=(channels // width,), in_specs=[spec] *...  16.6 us
    all_to_all x1, starting transfers between devices, expert_layer(): lax.all_to_all(send_rows, 'ep', split_axis=0, concat_axis=0, tiled=True)  6.35 us
    all_to_all x1, starting transfers between devices, expert_layer(): lax.all_to_all(result.transpose(1, 0, 2, 3).reshape(expert_count, busiest...  4.64 us
    dot_general x1, matrix products, expert_layer(): jnp.dot(flat_rows, specialist_valve_matrix[0], preferred_element_type=jnp...  3.82 us
    dot_general x1, matrix products, finish(): jnp.dot(collect(mixed_rows, 1, 3, 'mixed_gather'), subspace_merge_matrix,...  3.78 us
    dot_general x1, matrix products, expert_layer(): jnp.dot(collect(hidden, 1, 2, 'hidden_gather'), specialist_lowering_matri...  3.43 us
    pallas_call x1, Pallas kernels, finish_part(): pl.pallas_call(finish_kernel, out_shape=jax.ShapeDtypeStruct((span, chann...  3.15 us
  transfers between devices with their start and end apart: 3, of which 0 were waited for; matrix products, arithmetic and copies ran while one was open for 13% of the time, Pallas kernels for 56%

profile of v1, /device:TPU:0, one launch (start us, length us, event | category | flops | bytes accessed | tf_op | source)
XLA Modules:
  0.0 109.2 jit_solution(1179679465950989521)
XLA Ops:
  7.2 0.7 and_select_fusion.1
  7.9 0.7 fusion.27
  8.5 1.2 %multiply_reduce_fusion = f32[64]{0:T(128)S(1)} fusion(bf16[64,4096]{1,0:T(8,128)(2,1)} %param.25), kind=kLoop, calls=%fused_computation.13 | loop fusion | flops 786368 | bytes 524544 | tf_op jit(solution)/shard_map/reduce_sum | solution.py:321
  9.8 0.2 convert_reduce_fusion
  10.0 0.7 multiply_add_fusion
  10.7 0.7 dynamic_slice.7
  11.4 1.2 %convolution_convert_fusion.1 = bf16[96,1024]{1,0:T(8,128)(2,1)S(1)} fusion(f32[1024]{0:T(1024)S(1)} %dynamic_slice.7, f32[64]{0:T(128)S(1)} %add_rsqrt_fusion, bf16[64,4096]{1,0:T(8,128)(2,1)} %param.25, s32[]{:T(128)S(6)} %select_n.29, s32[64]{0:T(128)S(1)} %multiply_add_fusion), kind=kOutput, calls=%fused_computation.10 | convolution fusion | flops 12949504 | bytes 332292 | tf_op jit(solution)/shard_map/dot_general | solution.py:332
  12.5 0.7 reshape.104
  13.3 6.4 %all-to-all-start = ((bf16[8,12,1024]{2,1,0:T(8,128)(2,1)}), bf16[8,12,1024]{2,1,0:T(8,128)(2,1)S(1)}, u32[]{:S(2)}, u32[]{:S(2)}) async-start(bf16[8,12,1024]{2,1,0:T(8,128)(2,1)} %reshape.104), calls=%async_computation | async-start | bytes 524288 | tf_op jit(solution)/shard_map/all_to_all | solution.py:337
  19.7 0.0 all-gather.3.cloned.1.call-start
  19.7 16.6 %local_part.1 = (f32[128,1024]{1,0:T(8,128)}, bf16[128,512]{1,0:T(8,128)(2,1)}) custom-call(bf16[128,512]{1,0:T(8,128)(2,1)} %r_ref, bf16[128,512]{1,0:T(8,128)(2,1)} %k_ref.1, bf16[128,512]{1,0:T(8,128)(2,1)} %v_ref.1, bf16[128,512]{1,0:T(8,128)(2,1)} %fix_ref.1, bf16[128,512]{1,0:T(8,128)(2,1)} %fade_ref.1, bf16[128,512]{1,0:T(8,128)(2,1)} %loss_ref.1, ...), custom_call_target="tpu_custom_call" | custom-call | flops 335544320 | bytes 1703936 | tf_op jit(solution)/shard_map/local_part/pallas_call | solution.py:129
  36.3 0.0 all-gather.3.cloned.1.call-update
  36.3 0.0 all-to-all-done
  36.3 0.7 reshape.105.x_ref
  37.0 16.1 %row_gather.1 = bf16[2,96,4096]{2,1,0:T(8,128)(2,1)} custom-call(bf16[96,1024]{1,0:T(8,128)(2,1)} %reshape.105.x_ref), custom_call_target="tpu_custom_call" | custom-call | bytes 12582912 | tf_op jit(solution)/shard_map/row_gather/pallas_call | solution.py:245
  53.1 0.0 copy-start
  53.1 0.0 copy-start.3
  53.1 3.8 %fusion.4 = f32[192,512]{1,0:T(8,128)S(1)} fusion(bf16[192,4096]{1,0:T(8,128)(2,1)} %bitcast.46, bf16[1,4096,512]{2,1,0:T(8,128)(2,1)} %param.29), kind=kOutput, calls=%fused_computation.4 | convolution fusion | flops 805306368 | bytes 6160384 | tf_op jit(solution)/shard_map/dot_general | solution.py:339
  57.0 0.0 copy-done
  57.0 0.6 copy-done.3
  57.6 1.7 %fusion.12.x_ref = bf16[192,512]{1,0:T(8,128)(2,1)} fusion(bf16[192,4096]{1,0:T(8,128)(2,1)S(1)} %bitcast.47, bf16[1,4096,512]{2,1,0:T(8,128)(2,1)S(1)} %copy-done.3, f32[192,512]{1,0:T(8,128)S(1)} %fusion.4), kind=kOutput, calls=%fused_computation.9 | convolution fusion | flops 805896192 | bytes 6356992 | tf_op jit(solution)/shard_map/dot_general | solution.py:340
  59.2 14.3 %hidden_gather.1 = bf16[1,192,2048]{2,1,0:T(8,128)(2,1)} custom-call(bf16[192,512]{1,0:T(8,128)(2,1)} %fusion.12.x_ref), custom_call_target="tpu_custom_call" | custom-call | bytes 6291456 | tf_op jit(solution)/shard_map/hidden_gather/pallas_call | solution.py:245
  73.5 0.0 copy-start.1
  73.5 0.0 copy-start.2
  73.5 3.4 %fusion.6 = bf16[192,1024]{1,0:T(8,128)(2,1)S(1)} fusion(bf16[1,2048,1024]{2,1,0:T(8,128)(2,1)} %param.31, bf16[1,192,2048]{2,1,0:T(8,128)(2,1)} %hidden_gather.1), kind=kOutput, calls=%fused_computation.6 | convolution fusion | flops 805502976 | bytes 5373952 | tf_op jit(solution)/shard_map/dot_general | solution.py:342
  76.9 0.1 reshape.108
  77.0 0.2 copy.29
  77.3 1.0 copy.30
  78.2 4.6 %all-to-all-start.1 = ((bf16[8,24,1024]{2,1,0:T(8,128)(2,1)}), bf16[8,24,1024]{2,1,0:T(8,128)(2,1)S(1)}, u32[]{:S(2)}, u32[]{:S(2)}) async-start(bf16[8,24,1024]{2,1,0:T(8,128)(2,1)} %copy.30), calls=%async_computation.1 | async-start | bytes 786432 | tf_op jit(solution)/shard_map/all_to_all | solution.py:350
  82.9 0.0 copy-done.1
  82.9 0.0 copy-done.2
  82.9 0.0 all-gather.3.cloned.1.call-done
  82.9 3.2 %finish_part.1.x_ref = bf16[128,512]{1,0:T(8,128)(2,1)} custom-call(f32[128,1024]{1,0:T(8,128)} %get-tuple-element.12.own_ref, bf16[8,128,512]{2,1,0:T(8,128)(2,1)} %bitcast.50, f32[1,512]{1,0:T(1,128)} %bitcast.51), custom_call_target="tpu_custom_call" | custom-call | flops 268435456 | bytes 8388608 | tf_op jit(solution)/shard_map/finish_part/pallas_call | solution.py:181
  86.1 11.4 %mixed_gather.1 = bf16[1,128,2048]{2,1,0:T(8,128)(2,1)} custom-call(bf16[128,512]{1,0:T(8,128)(2,1)} %finish_part.1.x_ref), custom_call_target="tpu_custom_call" | custom-call | bytes 4194304 | tf_op jit(solution)/shard_map/mixed_gather/pallas_call | solution.py:245
  97.5 3.8 %convolution_convert_fusion = bf16[128,1024]{1,0:T(8,128)(2,1)} fusion(bf16[2048,1024]{1,0:T(8,128)(2,1)} %param.24, bf16[1,128,2048]{2,1,0:T(8,128)(2,1)} %mixed_gather.1), kind=kOutput, calls=%fused_computation.8 | convolution fusion | flops 537001984 | bytes 4980736 | tf_op jit(solution)/shard_map/dot_general | solution.py:294
  101.3 0.0 all-to-all-done.1
  101.3 1.0 fusion.15
  (3 shorter events, 0.0 us)
Async XLA Ops:
  13.3 23.0 %all-to-all-start = ((bf16[8,12,1024]{2,1,0:T(8,128)(2,1)}), bf16[8,12,1024]{2,1,0:T(8,128)(2,1)S(1)}, u32[]{:S(2)}, u32[]{:S(2)}) async-start(bf16[8,12,1024]{2,1,0:T(8,128)(2,1)} %reshape.104), calls=%async_computation | async-start | bytes 524288 | tf_op jit(solution)/shard_map/all_to_all | solution.py:337
  19.7 63.3 %all-gather.3.cloned.1.call-start = ((), (), s32[]{:S(2)}) async-start(), calls=%async_computation.2 | async-start | bytes 1179648 | tf_op jit(solution)/shard_map/all_gather | solution.py:289
  53.1 3.9 %copy-start = (bf16[2,96,4096]{2,1,0:T(8,128)(2,1)S(1)}, bf16[2,96,4096]{2,1,0:T(8,128)(2,1)}, u32[]{:S(2)}) copy-start(bf16[2,96,4096]{2,1,0:T(8,128)(2,1)} %row_gather.1) | copy-start | bytes 4718596
  53.1 4.4 %copy-start.3 = (bf16[1,4096,512]{2,1,0:T(8,128)(2,1)S(1)}, bf16[1,4096,512]{2,1,0:T(8,128)(2,1)}, u32[]{:S(2)}) copy-start(bf16[1,4096,512]{2,1,0:T(8,128)(2,1)} %param.30) | copy-start | bytes 12582916
  73.5 9.4 %copy-start.1 = (s32[64,2]{0,1:T(2,128)S(1)}, s32[64,2]{0,1:T(2,128)}, u32[]{:S(2)}) copy-start(s32[64,2]{0,1:T(2,128)} %param.27) | copy-start | bytes 1540
  73.5 9.4 %copy-start.2 = (f32[64,2]{0,1:T(2,128)S(1)}, f32[64,2]{0,1:T(2,128)}, u32[]{:S(2)}) copy-start(f32[64,2]{0,1:T(2,128)} %param.28) | copy-start | bytes 1540
  78.2 23.0 %all-to-all-start.1 = ((bf16[8,24,1024]{2,1,0:T(8,128)(2,1)}), bf16[8,24,1024]{2,1,0:T(8,128)(2,1)S(1)}, u32[]{:S(2)}, u32[]{:S(2)}) async-start(bf16[8,24,1024]{2,1,0:T(8,128)(2,1)} %copy.30), calls=%async_computation.1 | async-start | bytes 786432 | tf_op jit(solution)/shard_map/all_to_all | solution.py:350
Sparse Core Ops, SparseCore 0:
  36.4 23.6 all-gather.2
